TPU v7x, 32 devices: a whole 2x2x4 slice. The times are simulated.
32 devices in a mesh: sp: 4 (over y, x), tp: 8 (over z, core).
Axes of the slice: x: 2, y: 2, z: 4, core: 2. Of those that a mesh axis runs over, the one named last changes fastest.
Arguments:
- skip_stream_entry: bfloat16 [2048, 2048], P(('sp', 'tp')), may hold values from -6 to 6
- result_switch_mapped: bfloat16 [2048, 4096], P('sp', 'tp'), may hold values from -6 to 6
- channel_feed_mapped: bfloat16 [2048, 4096], P('sp', 'tp'), may hold values from -6 to 6
- write_coefficient_mapped: bfloat16 [2048, 2048], P('sp', 'tp'), may hold values from -6 to 6
- emission_coefficient_mapped: bfloat16 [2048, 2048], P('sp', 'tp'), may hold values from -6 to 6
- channel_feed_taps: bfloat16 [5, 4096], P(None, 'tp'), may hold values from -2.5 to 2.5
- write_coefficient_taps: bfloat16 [5, 2048], P(None, 'tp'), may hold values from -2.5 to 2.5
- emission_coefficient_taps: bfloat16 [5, 2048], P(None, 'tp'), may hold values from -2.5 to 2.5
- raw_increments: bfloat16 [2, 64, 2048], P(None, 'tp', 'sp'), may hold values from -6 to 6
- channel_log_fade_speed: float32 [2, 64], P(None, 'tp'), may hold values from -20 to 0
- extra_log_fade: float32 [2, 64, 2048], P(None, 'tp', 'sp'), may hold values from -1 to 0
- cluster_scaling_factor: float32 [4096], P('tp'), may hold values from 0.1 to 1.9
- blend_result_matrix: bfloat16 [4096, 2048], P('tp'), may hold values from -0.09375 to 0.09375
- routing_scaling_factor: float32 [2048], replicated, may hold values from 0.1 to 1.9
- specialist_switch_matrix: bfloat16 [8, 2048, 4096], P('sp', None, 'tp'), may hold values from -0.125 to 0.125
- specialist_widen_matrix: bfloat16 [8, 2048, 4096], P('sp', None, 'tp'), may hold values from -0.125 to 0.125
- specialist_contract_matrix: bfloat16 [8, 4096, 2048], P('sp', 'tp'), may hold values from -0.1875 to 0.1875
- picked_specialists: int32 [2048, 2], P(('sp', 'tp')), may hold values from 0 to 7, all different within a row; in each aligned block of 64 rows (0 to 63, 64 to 127, ...) at most 24 rows name the same one
- router_affinities: float32 [2048, 2], P(('sp', 'tp')), may hold values from 0.1 to 1
Outputs:
- result: bfloat16 [2048, 2048], P(('sp', 'tp'))
Inputs may be any that keep to these rules, and one draw needn't show every extreme that they name: `picked_specialists`: each row names 2 different experts. Within the rows of one device (aligned blocks of 64 rows) no expert is named more than 24 times, a bound that some block reaches.
All inputs are finite; a program needn't handle non-finite values.
Results may differ from a plain program's by a relative error of at most 0.02.
Values may be sent and summed in bfloat16 or wider, within the bound.
No kernel may reach another device: no remote copies, remote signals or barrier semaphores. Data moves between devices by JAX's collectives and lax.ppermute only.
A program may use at most 64 MiB of HBM per device.

v0:
```python
import jax
import jax.numpy as jnp
from jax import lax
from jax.sharding import PartitionSpec as P

WIDTH = 2048
HEAD_DIM = 64
GROUPS = 16
STATE = 128
CONV_W = 5
BLOCK = 128
TOP = 2
INNER = 4096
EPSILON = 1e-06
HIGHEST_MODE = lax.Precision.HIGHEST


def with_halo(block, sides, width):
    for axis, dim in sides:
        count = lax.axis_size(axis)
        forward = [(i, i + 1) for i in range(count - 1)]
        backward = [(target, source) for source, target in forward]
        low = lax.ppermute(
            lax.slice_in_dim(block, block.shape[dim] - width, None, axis=dim), axis, forward
        )
        high = lax.ppermute(lax.slice_in_dim(block, 0, width, axis=dim), axis, backward)
        block = jnp.concatenate([low, block, high], axis=dim)
    return block


def prefix(shard, axis, combine, identity, reverse):
    peers, here = (lax.axis_size(axis), lax.axis_index(axis))
    everything = jax.tree.map(
        lambda part, kind: lax.all_gather(part.astype(kind), axis),
        shard,
        (jnp.bfloat16, jnp.bfloat16),
    )
    start = jax.tree.map(
        lambda part, zero: jnp.broadcast_to(jnp.asarray(zero, part.dtype), part.shape),
        shard,
        identity,
    )

    def hop(k, before):
        at = peers - 1 - k if reverse else k
        reached = at > here if reverse else at < here
        new = combine(
            before, jax.tree.map(lambda part, own: part[at].astype(own.dtype), everything, shard)
        )
        return jax.tree.map(lambda a, b: jnp.where(reached, a, b), new, before)

    return lax.fori_loop(0, peers, hop, start)


def centred_conv(padded, weights, series_count):
    summed = jnp.zeros((series_count, padded.shape[1]), jnp.float32)
    for offset in range(weights.shape[0]):
        summed = summed + weights[offset].astype(jnp.float32) * padded[
            offset : offset + series_count
        ].astype(jnp.float32)
    return jax.nn.silu(summed)


def local_sweep(inputs, entry_state, readout_state, log_fade_factor, softplus_increment):
    seq_len = inputs.shape[0]
    blocks = seq_len // BLOCK
    heads_here = log_fade_factor.shape[0]
    groups_here = entry_state.shape[1] // STATE
    per_group = heads_here // groups_here
    values = inputs.reshape(blocks, BLOCK, groups_here, per_group, HEAD_DIM)
    b_blocks = entry_state.reshape(blocks, BLOCK, groups_here, STATE)
    c_blocks = readout_state.reshape(blocks, BLOCK, groups_here, STATE)
    decay_blocks = log_fade_factor.reshape(groups_here, per_group, blocks, BLOCK)
    step_blocks = softplus_increment.reshape(groups_here, per_group, blocks, BLOCK)
    cumulative = jnp.cumsum(decay_blocks, axis=-1)
    group_inner = jnp.einsum("bign,bjgn->gbij", c_blocks, b_blocks, precision=HIGHEST_MODE)
    spread = cumulative[..., :, None] - cumulative[..., None, :]
    lower_tri = jnp.arange(BLOCK)[:, None] >= jnp.arange(BLOCK)[None, :]
    mixing = (
        jnp.exp(jnp.where(lower_tri, spread, -jnp.inf))
        * step_blocks[..., None, :]
        * group_inner[:, None]
    )
    within = jnp.einsum("gkbij,bjgkp->bigkp", mixing, values, precision=HIGHEST_MODE)
    to_end = jnp.exp(cumulative[..., -1:] - cumulative) * step_blocks
    block_states = jnp.einsum(
        "gkbj,bjgkp,bjgn->bgkpn", to_end, values, b_blocks, precision=HIGHEST_MODE
    )
    block_decay = cumulative[..., -1]

    def advance(carried, pieces):
        state_piece, decay_piece = pieces
        return (carried * jnp.exp(decay_piece)[..., None, None] + state_piece, carried)

    zero_state = jnp.zeros((groups_here, per_group, HEAD_DIM, STATE), jnp.float32)
    final_state, entering = lax.scan(
        advance, zero_state, (block_states, jnp.moveaxis(block_decay, -1, 0))
    )
    before = jnp.cumsum(block_decay, axis=-1) - block_decay
    return (
        (within, entering, cumulative, before, c_blocks),
        (jnp.sum(block_decay, axis=-1), final_state),
    )


def finish_sweep(parts, carried):
    within, entering, cumulative, before, c_blocks = parts
    entering = entering + carried[None] * jnp.exp(jnp.moveaxis(before, -1, 0))[..., None, None]
    readout = jnp.einsum("bign,bgkpn->bigkp", c_blocks, entering, precision=HIGHEST_MODE)
    readout = readout * jnp.exp(jnp.transpose(cumulative, (2, 3, 0, 1)))[..., None]
    combined = within + readout
    return combined.reshape(combined.shape[0] * combined.shape[1], -1)


def blend_parts_list(
    channel_feed_bordered,
    write_coefficient_bordered,
    emission_coefficient_bordered,
    channel_feed_taps,
    write_coefficient_taps,
    emission_coefficient_taps,
    raw_increments,
    channel_log_fade_speed,
    extra_log_fade,
    series_count,
):
    inputs = centred_conv(channel_feed_bordered, channel_feed_taps, series_count)
    entry_state = centred_conv(write_coefficient_bordered, write_coefficient_taps, series_count)
    readout_state = centred_conv(
        emission_coefficient_bordered, emission_coefficient_taps, series_count
    )
    softplus_increment = jax.nn.softplus(raw_increments.astype(jnp.float32))
    log_fade_factor = (
        -softplus_increment * jnp.exp(channel_log_fade_speed)[..., None] + extra_log_fade
    )
    onward_pass = local_sweep(
        inputs, entry_state, readout_state, log_fade_factor[0], softplus_increment[0]
    )
    backward_pass = local_sweep(
        jnp.flip(inputs, 0),
        jnp.flip(entry_state, 0),
        jnp.flip(readout_state, 0),
        jnp.flip(log_fade_factor[1], -1),
        jnp.flip(softplus_increment[1], -1),
    )
    return (onward_pass, backward_pass)


def gated_norm(mixed_sum, result_switch_mapped, cluster_scaling_factor):
    gated = mixed_sum * jax.nn.silu(result_switch_mapped.astype(jnp.float32))
    grouped = gated.reshape(gated.shape[0], -1, INNER // GROUPS)
    normalized = grouped * lax.rsqrt(jnp.mean(grouped * grouped, axis=-1, keepdims=True) + EPSILON)
    return (normalized.reshape(gated.shape) * cluster_scaling_factor).astype(jnp.bfloat16)


def rms_scale(stream, gain):
    values = stream.astype(jnp.float32)
    return (
        values * lax.rsqrt(jnp.mean(values * values, axis=-1, keepdims=True) + EPSILON) * gain
    ).astype(jnp.bfloat16)


def link_states(former, latter):
    former_total, former_state = former
    latter_total, latter_state = latter
    return (
        former_total + latter_total,
        former_state * jnp.exp(latter_total)[..., None, None] + latter_state,
    )


def per_device(
    skip_stream_entry,
    result_switch_mapped,
    channel_feed_mapped,
    write_coefficient_mapped,
    emission_coefficient_mapped,
    channel_feed_taps,
    write_coefficient_taps,
    emission_coefficient_taps,
    raw_increments,
    channel_log_fade_speed,
    extra_log_fade,
    cluster_scaling_factor,
    blend_result_matrix,
    routing_scaling_factor,
    specialist_switch_matrix,
    specialist_widen_matrix,
    specialist_contract_matrix,
    picked_specialists,
    router_affinities,
):
    series_count = channel_feed_mapped.shape[0]
    rim_width = CONV_W // 2
    sources = (channel_feed_mapped, write_coefficient_mapped, emission_coefficient_mapped)
    edges = jnp.concatenate(
        [jnp.concatenate([source[:rim_width], source[-rim_width:]], 0) for source in sources], 1
    )
    rimmed = with_halo(edges, (("sp", 0),), rim_width)
    padded_list = []
    column_start = 0
    for source in sources:
        width_here = source.shape[1]
        upper_rim = rimmed[:rim_width, column_start : column_start + width_here]
        lower_rim = rimmed[-rim_width:, column_start : column_start + width_here]
        padded_list.append(jnp.concatenate([upper_rim, source, lower_rim], 0))
        column_start = column_start + width_here
    onward_pass, backward_pass = blend_parts_list(
        padded_list[0],
        padded_list[1],
        padded_list[2],
        channel_feed_taps,
        write_coefficient_taps,
        emission_coefficient_taps,
        raw_increments,
        channel_log_fade_speed,
        extra_log_fade,
        series_count,
    )
    fwd_total, fwd_final = onward_pass[1]
    bwd_total, bwd_final = backward_pass[1]
    identity_pair = (jnp.zeros_like(fwd_total), jnp.zeros_like(fwd_final))
    carried_fwd = prefix((fwd_total, fwd_final), "sp", link_states, identity_pair, False)[1]
    carried_bwd = prefix((bwd_total, bwd_final), "sp", link_states, identity_pair, True)[1]
    mixed_sum = finish_sweep(onward_pass[0], carried_fwd) + jnp.flip(
        finish_sweep(backward_pass[0], carried_bwd), 0
    )
    mixed_rows = gated_norm(mixed_sum, result_switch_mapped, cluster_scaling_factor)
    rows_here = skip_stream_entry.shape[0]
    projected = lax.psum_scatter(
        jnp.dot(mixed_rows, blend_result_matrix, preferred_element_type=jnp.float32).astype(
            jnp.bfloat16
        ),
        "tp",
        scatter_dimension=0,
        tiled=True,
    ).astype(jnp.float32)
    after_mixer = (skip_stream_entry.astype(jnp.float32) + projected).astype(jnp.bfloat16)
    normed = rms_scale(after_mixer, routing_scaling_factor)
    experts_here = specialist_switch_matrix.shape[0]
    expert_count = experts_here * lax.axis_size("sp")
    capacity = max(2, 3 * TOP * rows_here // (2 * expert_count))
    slot_total = capacity * expert_count
    flat_routes = picked_specialists.reshape(-1)
    one_hot = (flat_routes[:, None] == jnp.arange(expert_count, dtype=jnp.int32)[None, :]).astype(
        jnp.int32
    )
    earlier_count = jnp.cumsum(one_hot, axis=0) - one_hot
    slot_rank = jnp.sum(earlier_count * one_hot, axis=1)
    position = slot_rank * expert_count + flat_routes
    slot_match = (position[:, None] == jnp.arange(slot_total, dtype=jnp.int32)[None, :]).astype(
        jnp.bfloat16
    )
    buffer = jnp.einsum(
        "rks,rd->sd",
        slot_match.reshape(rows_here, TOP, slot_total),
        normed,
        preferred_element_type=jnp.float32,
    ).astype(jnp.bfloat16)
    buffer = buffer.reshape(capacity, expert_count, WIDTH)
    received = lax.all_to_all(buffer, "sp", split_axis=1, concat_axis=0, tiled=True)
    data_block = lax.all_gather(received, "tp", axis=0, tiled=True)
    gate_part = jnp.einsum(
        "red,edf->ref", data_block, specialist_switch_matrix, preferred_element_type=jnp.float32
    )
    up_part = jnp.einsum(
        "red,edf->ref", data_block, specialist_widen_matrix, preferred_element_type=jnp.float32
    )
    hidden = (jax.nn.silu(gate_part) * up_part).astype(jnp.bfloat16)
    expert_out = lax.psum_scatter(
        jnp.einsum(
            "ref,efd->red", hidden, specialist_contract_matrix, preferred_element_type=jnp.float32
        ).astype(jnp.bfloat16),
        "tp",
        scatter_dimension=0,
        tiled=True,
    )
    returned = lax.all_to_all(expert_out, "sp", split_axis=0, concat_axis=1, tiled=True)
    picked = jnp.dot(
        slot_match, returned.reshape(slot_total, WIDTH), preferred_element_type=jnp.float32
    )
    weights = router_affinities / jnp.sum(router_affinities, axis=-1, keepdims=True)
    mixture = jnp.sum(weights[..., None] * picked.reshape(rows_here, TOP, WIDTH), axis=1)
    return (after_mixer.astype(jnp.float32) + mixture).astype(jnp.bfloat16)


def solution(mesh):
    in_specs = (
        P(("sp", "tp"), None),
        P("sp", "tp"),
        P("sp", "tp"),
        P("sp", "tp"),
        P("sp", "tp"),
        P(None, "tp"),
        P(None, "tp"),
        P(None, "tp"),
        P(None, "tp", "sp"),
        P(None, "tp"),
        P(None, "tp", "sp"),
        P("tp"),
        P("tp", None),
        P(),
        P("sp", None, "tp"),
        P("sp", None, "tp"),
        P("sp", "tp", None),
        P(("sp", "tp"), None),
        P(("sp", "tp"), None),
    )
    out_specs = P(("sp", "tp"), None)
    return jax.shard_map(
        per_device, mesh=mesh, in_specs=in_specs, out_specs=out_specs, check_vma=False
    )
```

profile of v0, /device:TPU:0, one launch (start us, length us, event | category | flops | bytes accessed | tf_op | source)
XLA Modules:
  0.0 437.1 jit_solution(5094532863845228223)
XLA Ops:
  9.1 5.6 %collective-permute-start = (bf16[2,1024]{0,1:T(8,128)(2,1)}, bf16[2,1024]{0,1:T(8,128)(2,1)}, u32[]{:S(2)}, u32[]{:S(2)}) collective-permute-start(bf16[2,1024]{0,1:T(8,128)(2,1)} %copy.175), channel_id=1, source_target_pairs={{0,8},{8,16},{16,24},{1,9},{9,17},{17,25},{2,10},{10,18},{18,26},{... | collective-permute-start | bytes 12296 | tf_op jit(solution)/shard_map/ppermute | solution.py:23
  19.8 1.5 slice_convert_fusion.4
  22.8 2.4 reduce_window_sum.45
  27.1 2.4 reduce_window_sum.47
  30.8 9.6 %all-gather.4 = bf16[4,2,4]{2,1,0:T(2,128)(2,1)} all-gather(bf16[1,2,4]{2,1,0:T(2,128)(2,1)S(1)} %bitcast.210), channel_id=2, replica_groups=mesh['sp'=4,'tp'=8] {'sp'}, dimensions={0}, use_global_device_ids=true | all-gather | bytes 80 | tf_op jit(solution)/shard_map/all_gather | solution.py:34
  40.5 8.3 %all-gather.5 = bf16[4,2,4]{2,1,0:T(2,128)(2,1)} all-gather(bf16[1,2,4]{2,1,0:T(2,128)(2,1)S(1)} %bitcast.211), channel_id=4, replica_groups=mesh['sp'=4,'tp'=8] {'sp'}, dimensions={0}, use_global_device_ids=true | all-gather | bytes 80 | tf_op jit(solution)/shard_map/all_gather | solution.py:34
  48.8 2.1 copy.176
  56.0 2.0 copy.210
  59.6 1.5 fusion.101
  61.1 1.5 copy.184
  62.6 2.0 divide_multiply_fusion.2
  64.6 2.1 reshape.175
  66.7 4.7 %rev.24 = f32[512,256]{1,0:T(8,128)} reverse(f32[512,256]{1,0:T(8,128)} %divide_multiply_fusion.2), dimensions={0} | reverse | bytes 1048576 | tf_op jit(solution)/shard_map/jit(_flip)/rev | solution.py:142
  71.7 3.1 divide_multiply_fusion.1
  74.7 2.1 reshape.176
  76.8 4.7 %rev.25 = f32[512,256]{1,0:T(8,128)} reverse(f32[512,256]{1,0:T(8,128)} %divide_multiply_fusion.1), dimensions={0} | reverse | bytes 1048576 | tf_op jit(solution)/shard_map/jit(_flip)/rev | solution.py:141
  83.4 4.7 %divide_multiply_fusion = f32[512,512]{0,1:T(8,128)} fusion(bf16[512,512]{0,1:T(8,128)(2,1)} %copy.176, bf16[2,512]{0,1:T(8,128)(2,1)S(1)} %slice.207, bf16[2,512]{0,1:T(8,128)(2,1)S(1)} %slice.203, f32[512]{0:T(512)S(1)} %bitcast.198, f32[512]{0:T(512)S(1)} %bitcast.199, f32[512]{0:T(512)S(1)} %bitcast.196, f32[512]{0:T(512)S(1)} %bitcast.197, ...), kind=kLoop, calls=%fused_computation.78 | loop fusion | flops 7864320 | bytes 1587200 | tf_op jit(solution)/shard_map/jit(silu)/mul | solution.py:61
  88.1 2.6 reshape.174
  90.7 9.4 %rev.21 = f32[512,512]{0,1:T(8,128)} reverse(f32[512,512]{0,1:T(8,128)} %divide_multiply_fusion), dimensions={0} | reverse | bytes 2097152 | tf_op jit(solution)/shard_map/jit(_flip)/rev | solution.py:140
  100.1 3.3 fusion.72
  104.8 2.1 fusion.40
  108.0 9.8 %while.56 = (s32[]{:T(128)}, f32[2,4,64,128]{3,2,1,0:T(8,128)S(1)}, f32[4,2,4,64,128]{4,3,2,1,0:T(8,128)}, f32[4,2,4]{2,1,0:T(2,128)}, f32[4,2,4,64,128]{4,3,2,1,0:T(8,128)}, /*index=5*/s32[]{:T(128)}, s32[]{:T(128)}) while((s32[]{:T(128)}, f32[2,4,64,128]{3,2,1,0:T(8,128)S(1)}, f32[4,2,4,64,128]{4,3,2,1,0:T(8,128)}, ...), condition=%wide.region_2.3_spmd.clone, body=%wide.region_1.2_spmd.clone.sunk | while | flops 262147 | bytes 1311424 | solution.py:96
  117.8 10.1 %all-gather.1 = bf16[8,4,64,128]{3,2,1,0:T(8,128)(2,1)} all-gather(bf16[2,4,64,128]{3,2,1,0:T(8,128)(2,1)S(1)} %convert_element_type.229), channel_id=3, replica_groups=mesh['sp'=4,'tp'=8] {'sp'}, dimensions={0}, use_global_device_ids=true | all-gather | bytes 655360 | tf_op jit(solution)/shard_map/all_gather | solution.py:34
  127.9 6.8 %while.57 = (s32[]{:T(128)}, f32[2,4,64,128]{3,2,1,0:T(8,128)S(1)}, s32[]{:T(128)}, bf16[4,2,4]{2,1,0:T(2,128)(2,1)}, bf16[4,2,4,64,128]{4,3,2,1,0:T(8,128)(2,1)}, /*index=5*/s32[]{:T(128)}, s32[]{:T(128)}) while((s32[]{:T(128)}, f32[2,4,64,128]{3,2,1,0:T(8,128)S(1)}, s32[]{:T(128)}, bf16[4,2,4]{2,1,0:T(2,128)(2,1)}, ...), condition=%wide.region_5.6_spmd.clone, body=%wide.region_4.5_spmd.clone.sunk | while | flops 327692 | bytes 655545 | solution.py:52
  134.8 5.6 %fusion.20 = f32[4,128,2,4,64]{1,4,3,2,0:T(8,128)S(1)} fusion(f32[4,128,2,4,64]{1,0,4,3,2:T(4,128)} %reshape.174, f32[2,4,128,128]{3,2,0,1:T(8,128)} %fusion.72, f32[2,4,4,128]{3,1,0,2:T(4,128)S(1)} %bitcast.194, f32[2,4,4,128]{3,1,0,2:T(4,128)S(1)} %copy-done.21, pred[128,128]{1,0:T(8,128)(4,1)S(1)} %copy-done.19), kind=kOutput, calls=%fused_computation.37 | convolution fusion | flops 404750336 | bytes 2670592 | tf_op jit(solution)/shard_map/gkbij,bjgkp->bigkp/dot_general | solution.py:84
  141.7 1.7 copy.196
  144.7 2.1 reshape.181
  146.9 2.5 reshape.178
  149.4 3.1 fusion.69
  153.9 2.1 fusion.37
  157.1 9.8 %while.58 = (s32[]{:T(128)}, f32[2,4,64,128]{3,2,1,0:T(8,128)S(1)}, f32[4,2,4,64,128]{4,3,2,1,0:T(8,128)}, f32[4,2,4]{2,1,0:T(2,128)}, f32[4,2,4,64,128]{4,3,2,1,0:T(8,128)}, /*index=5*/s32[]{:T(128)}, s32[]{:T(128)}) while((s32[]{:T(128)}, f32[2,4,64,128]{3,2,1,0:T(8,128)S(1)}, f32[4,2,4,64,128]{4,3,2,1,0:T(8,128)}, ...), condition=%wide.region_9.10_spmd.clone, body=%wide.region_8.9_spmd.clone.sunk | while | flops 262147 | bytes 1311424 | solution.py:96
  166.9 10.7 %all-gather.3 = bf16[8,4,64,128]{3,2,1,0:T(8,128)(2,1)} all-gather(bf16[2,4,64,128]{3,2,1,0:T(8,128)(2,1)S(1)} %convert_element_type.232), channel_id=5, replica_groups=mesh['sp'=4,'tp'=8] {'sp'}, dimensions={0}, use_global_device_ids=true | all-gather | bytes 655360 | tf_op jit(solution)/shard_map/all_gather | solution.py:34
  177.6 6.8 %while.59 = (s32[]{:T(128)}, f32[2,4,64,128]{3,2,1,0:T(8,128)S(1)}, s32[]{:T(128)}, bf16[4,2,4]{2,1,0:T(2,128)(2,1)}, bf16[4,2,4,64,128]{4,3,2,1,0:T(8,128)(2,1)...) while((s32[]{:T(128)}, f32[2,4,64,128]{3,2,1,0:T(8,128)S(1)}, s32[]{:T(128)}, ...), condition=%wide.region_12.13_spmd.clone, body=%wide.region_11.12_spmd.clone.sunk | while | flops 327696 | bytes 655607 | solution.py:52
  184.4 5.6 %fusion.23 = f32[4,128,2,4,64]{1,4,3,2,0:T(8,128)S(1)} fusion(f32[4,128,2,4,64]{1,0,4,3,2:T(4,128)} %reshape.178, f32[2,4,128,128]{3,2,0,1:T(8,128)} %fusion.69, f32[2,4,4,128]{3,1,0,2:T(4,128)S(1)} %bitcast.193, f32[2,4,4,128]{3,1,0,2:T(4,128)S(1)} %copy-done.20, pred[128,128]{1,0:T(8,128)(4,1)S(1)} %copy-done.19), kind=kOutput, calls=%fused_computation.38 | convolution fusion | flops 404750336 | bytes 2670592 | tf_op jit(solution)/shard_map/gkbij,bjgkp->bigkp/dot_general | solution.py:84
  192.1 6.0 %rev.26 = f32[512,512]{0,1:T(8,128)} reverse(f32[512,512]{0,1:T(8,128)S(1)} %bitcast.183), dimensions={0} | reverse | bytes 2097152 | tf_op jit(solution)/shard_map/jit(_flip)/rev | solution.py:225
  198.1 2.1 bitcast_reduce_fusion
  200.5 2.6 convolution_convert_fusion
  204.2 35.4 %reduce-scatter.3.cloned.1.call-done = bf16[64,2048]{1,0:T(8,128)(2,1)} async-done(((bf16[512,2048]{1,0:T(8,128)(2,1)}), bf16[64,2048]{1,0:T(8,128)(2,1)}) %reduce-scatter.3.cloned.1.call-update) | async-done | bytes 262160 | tf_op jit(solution)/shard_map/reduce_scatter | solution.py:230
  242.6 12.0 %all_to_all.33 = bf16[24,8,2048]{2,0,1:T(8,128)(2,1)S(1)} all-to-all(bf16[24,8,2048]{2,0,1:T(8,128)(2,1)S(1)} %copy.213), channel_id=1, replica_groups=mesh['sp'=4,'tp'=8] {'sp'}, dimensions={1} | all-to-all | bytes 1572864 | tf_op jit(solution)/shard_map/all_to_all | solution.py:261
  255.9 63.8 %all-gather.8.cloned.1.call-done = bf16[768,2,2048]{2,0,1:T(8,128)(2,1)} async-done(((bf16[96,2,2048]{2,0,1:T(8,128)(2,1)}), bf16[768,2,2048]{2,0,1:T(8,128)(2,1)}) %all-gather.8.cloned.1.call-update) | async-done | bytes 6291472 | tf_op jit(solution)/shard_map/all_gather | solution.py:262
  319.7 9.1 %fusion.107 = f32[2,768,512]{2,1,0:T(8,128)} fusion(bf16[768,2,2048]{2,0,1:T(8,128)(2,1)} %all-gather.8.cloned.1.call-done, bf16[2,2048,512]{2,1,0:T(8,128)(2,1)} %param.42), kind=kOutput, calls=%fused_computation.197 | convolution fusion | flops 3221225472 | bytes 13631488 | tf_op jit(solution)/shard_map/red,edf->ref/dot_general | solution.py:266
  328.7 12.5 %convert_bitcast_fusion = bf16[768,2,2048]{2,0,1:T(8,128)(2,1)} fusion(bf16[2,512,2048]{2,1,0:T(8,128)(2,1)} %param.43, f32[2,768,512]{2,1,0:T(8,128)} %fusion.107, bf16[768,2,2048]{2,0,1:T(8,128)(2,1)} %all-gather.8.cloned.1.call-done, bf16[2,2048,512]{2,1,0:T(8,128)(2,1)} %param.41), kind=kOutput, calls=%fused_computation.12 | convolution fusion | flops 6450315264 | bytes 24117248 | tf_op jit(solution)/shard_map/ref,efd->red/dot_general | solution.py:271
  341.2 68.5 %reduce-scatter.5.cloned.1.call-done = bf16[96,2,2048]{2,0,1:T(8,128)(2,1)} async-done(((bf16[768,2,2048]{2,0,1:T(8,128)(2,1)}), bf16[96,2,2048]{2,0,1:T(8,128)(2,1)}) %reduce-scatter.5.cloned.1.call-update) | async-done | bytes 786448 | tf_op jit(solution)/shard_map/reduce_scatter | solution.py:270
  409.8 2.8 copy.215
  412.6 3.8 all-to-all-start.1
  416.4 9.1 %all-to-all-done.1 = bf16[96,2,2048]{2,1,0:T(2,128)(2,1)S(1)} async-done(((bf16[96,2,2048]{2,1,0:T(2,128)(2,1)}), bf16[96,2,2048]{2,1,0:T(2,128)(2,1)S(1)}, u32[]{:S(2)}, u32[]{:S(2)}) %all-to-all-start.1) | async-done | bytes 786464 | tf_op jit(solution)/shard_map/all_to_all | solution.py:278
  425.5 1.7 copy.260
  427.2 2.3 reshape.218
  (187 shorter events, 70.2 us)
Async XLA Ops:
  6.5 193.9 %copy-start = (bf16[512,2048]{1,0:T(8,128)(2,1)S(1)}, bf16[512,2048]{1,0:T(8,128)(2,1)}, u32[]{:S(2)}) copy-start(bf16[512,2048]{1,0:T(8,128)(2,1)} %param.39) | copy-start | bytes 6291460
  6.5 56.1 %copy-start.9 = (bf16[512,256]{1,0:T(8,128)(2,1)S(1)}, bf16[512,256]{1,0:T(8,128)(2,1)}, u32[]{:S(2)}) copy-start(bf16[512,256]{1,0:T(8,128)(2,1)} %param.31) | copy-start | bytes 786436
  6.5 233.0 %reduce-scatter.3.cloned.1.call-start = ((), (), s32[]{:S(2)}) async-start(), calls=%async_computation.4 | async-start | bytes 2359296 | tf_op jit(solution)/shard_map/reduce_scatter | solution.py:230
  9.1 49.0 %collective-permute-start = (bf16[2,1024]{0,1:T(8,128)(2,1)}, bf16[2,1024]{0,1:T(8,128)(2,1)}, u32[]{:S(2)}, u32[]{:S(2)}) collective-permute-start(bf16[2,1024]{0,1:T(8,128)(2,1)} %copy.175), channel_id=1, source_target_pairs={{0,8},{8,16},{16,24},{1,9},{9,17},{17,25},{2,10},{10,18},{18,26},{... | collective-permute-start | bytes 12296 | tf_op jit(solution)/shard_map/ppermute | solution.py:23
  15.5 44.0 %collective-permute-start.1 = (bf16[2,1024]{0,1:T(8,128)(2,1)}, bf16[2,1024]{0,1:T(8,128)(2,1)}, u32[]{:S(2)}, u32[]{:S(2)}) collective-permute-start(bf16[2,1024]{0,1:T(8,128)(2,1)} %copy.178), channel_id=1, source_target_pairs={{8,0},{16,8},{24,16},{9,1},{17,9},{25,17},{10,2},{18,10},{26,18},{... | collective-permute-start | bytes 12296 | tf_op jit(solution)/shard_map/ppermute | solution.py:26
  22.8 3.7 copy-start.15
  27.1 2.6 copy-start.13
  64.5 18.8 %copy-start.23 = (f32[1,512]{1,0:T(1,128)S(1)}, f32[1,512]{1,0:T(1,128)}, u32[]{:S(2)}) copy-start(f32[1,512]{1,0:T(1,128)} %get-tuple-element.481) | copy-start | bytes 6148
  64.5 18.9 %copy-start.24 = (f32[1,512]{1,0:T(1,128)S(1)}, f32[1,512]{1,0:T(1,128)}, u32[]{:S(2)}) copy-start(f32[1,512]{1,0:T(1,128)} %get-tuple-element.482) | copy-start | bytes 6148
  64.6 18.9 %copy-start.25 = (f32[1,512]{1,0:T(1,128)S(1)}, f32[1,512]{1,0:T(1,128)}, u32[]{:S(2)}) copy-start(f32[1,512]{1,0:T(1,128)} %get-tuple-element.483) | copy-start | bytes 6148
  64.6 18.9 %copy-start.26 = (f32[1,512]{1,0:T(1,128)S(1)}, f32[1,512]{1,0:T(1,128)}, u32[]{:S(2)}) copy-start(f32[1,512]{1,0:T(1,128)} %get-tuple-element.484) | copy-start | bytes 6148
  64.6 18.9 %copy-start.27 = (f32[1,512]{1,0:T(1,128)S(1)}, f32[1,512]{1,0:T(1,128)}, u32[]{:S(2)}) copy-start(f32[1,512]{1,0:T(1,128)} %get-tuple-element.485) | copy-start | bytes 6148
  88.1 15.3 %copy-start.10 = (f32[4,128,2,4]{1,0,3,2:T(4,128)S(1)}, f32[4,128,2,4]{1,0,3,2:T(4,128)}, u32[]{:S(2)}) copy-start(f32[4,128,2,4]{1,0,3,2:T(4,128)} %get-tuple-element.476) | copy-start | bytes 49156
  100.1 4.7 %copy-start.3 = (f32[4,128,2,128]{3,2,1,0:T(2,128)S(1)}, f32[4,128,2,128]{3,2,1,0:T(2,128)}, u32[]{:S(2)}) copy-start(f32[4,128,2,128]{3,2,1,0:T(2,128)} %reshape.176) | copy-start | bytes 1572868
  117.8 17.0 %copy-start.16 = (f32[1,8,512]{2,1,0:T(8,128)S(1)}, f32[1,8,512]{2,1,0:T(8,128)}, u32[]{:S(2)}) copy-start(f32[1,8,512]{2,1,0:T(8,128)} %copy-done.15) | copy-start | bytes 49156
  117.8 17.0 %copy-start.19 = (pred[128,128]{1,0:T(8,128)(4,1)S(1)}, pred[128,128]{1,0:T(8,128)(4,1)}, u32[]{:S(2)}) copy-start(pred[128,128]{1,0:T(8,128)(4,1)} %iota_compare_fusion.3) | copy-start | bytes 49156
  117.8 17.0 %copy-start.21 = (f32[2,4,4,128]{3,1,0,2:T(4,128)S(1)}, f32[2,4,4,128]{3,1,0,2:T(4,128)}, u32[]{:S(2)}) copy-start(f32[2,4,4,128]{3,1,0,2:T(4,128)} %copy.180) | copy-start | bytes 49156
  127.9 12.5 %copy-start.2 = (f32[4,128,2,128]{3,2,1,0:T(2,128)S(1)}, f32[4,128,2,128]{3,2,1,0:T(2,128)}, u32[]{:S(2)}) copy-start(f32[4,128,2,128]{3,2,1,0:T(2,128)} %reshape.175) | copy-start | bytes 1572868
  127.9 12.5 %copy-start.12 = (f32[4,128,2,4]{1,3,2,0:T(4,128)S(1)}, f32[4,128,2,4]{1,3,2,0:T(4,128)}, u32[]{:S(2)}) copy-start(f32[4,128,2,4]{1,3,2,0:T(4,128)} %copy.195) | copy-start | bytes 49156
  127.9 12.5 %copy-start.18 = (f32[4,2,4]{2,1,0:T(2,128)S(1)}, f32[4,2,4]{2,1,0:T(2,128)}, u32[]{:S(2)}) copy-start(f32[4,2,4]{2,1,0:T(2,128)} %copy.193) | copy-start | bytes 388
  134.7 5.7 %copy-start.5 = (f32[4,2,4,64,128]{4,3,2,1,0:T(8,128)S(1)}, f32[4,2,4,64,128]{4,3,2,1,0:T(8,128)}, u32[]{:S(2)}) copy-start(f32[4,2,4,64,128]{4,3,2,1,0:T(8,128)} %get-tuple-element.287) | copy-start | bytes 3145732
  149.4 4.5 %copy-start.4 = (f32[4,128,2,128]{3,2,1,0:T(2,128)S(1)}, f32[4,128,2,128]{3,2,1,0:T(2,128)}, u32[]{:S(2)}) copy-start(f32[4,128,2,128]{3,2,1,0:T(2,128)} %reshape.181) | copy-start | bytes 1572868
  166.9 17.5 %copy-start.14 = (f32[8,512]{1,0:T(8,128)S(1)}, f32[8,512]{1,0:T(8,128)}, u32[]{:S(2)}) copy-start(f32[8,512]{1,0:T(8,128)} %copy-done.13) | copy-start | bytes 49156
  166.9 17.5 %copy-start.20 = (f32[2,4,4,128]{3,1,0,2:T(4,128)S(1)}, f32[2,4,4,128]{3,1,0,2:T(4,128)}, u32[]{:S(2)}) copy-start(f32[2,4,4,128]{3,1,0,2:T(4,128)} %copy.197) | copy-start | bytes 49156
  177.6 12.5 %copy-start.11 = (f32[4,128,2,4]{1,3,2,0:T(4,128)S(1)}, f32[4,128,2,4]{1,3,2,0:T(4,128)}, u32[]{:S(2)}) copy-start(f32[4,128,2,4]{1,3,2,0:T(4,128)} %copy.208) | copy-start | bytes 49156
  177.6 12.5 %copy-start.17 = (f32[4,2,4]{2,1,0:T(2,128)S(1)}, f32[4,2,4]{2,1,0:T(2,128)}, u32[]{:S(2)}) copy-start(f32[4,2,4]{2,1,0:T(2,128)} %copy.206) | copy-start | bytes 388
  184.4 5.7 %copy-start.6 = (f32[4,2,4,64,128]{4,3,2,1,0:T(8,128)S(1)}, f32[4,2,4,64,128]{4,3,2,1,0:T(8,128)}, u32[]{:S(2)}) copy-start(f32[4,2,4,64,128]{4,3,2,1,0:T(8,128)} %get-tuple-element.290) | copy-start | bytes 3145732
  192.1 8.1 %copy-start.30 = (f32[512]{0:T(512)S(1)}, f32[512]{0:T(512)}, u32[]{:S(2)}) copy-start(f32[512]{0:T(512)} %param.38) | copy-start | bytes 6148
  200.4 2.7 copy-start.28
  200.5 39.1 %copy-start.7 = (bf16[64,2048]{1,0:T(8,128)(2,1)S(1)}, bf16[64,2048]{1,0:T(8,128)(2,1)}, u32[]{:S(2)}) copy-start(bf16[64,2048]{1,0:T(8,128)(2,1)} %param.27) | copy-start | bytes 786436
  200.5 40.3 %copy-start.22 = (f32[2048]{0:T(1024)S(1)}, f32[2048]{0:T(1024)}, u32[]{:S(2)}) copy-start(f32[2048]{0:T(1024)} %param.40) | copy-start | bytes 24580
  203.1 116.5 %all-gather.8.cloned.1.call-start = ((), (), s32[]{:S(2)}) async-start(), calls=%async_computation.5 | async-start | bytes 7077888 | tf_op jit(solution)/shard_map/all_gather | solution.py:262
  255.6 154.2 %reduce-scatter.5.cloned.1.call-start = ((), (), s32[]{:S(2)}) async-start(), calls=%async_computation.6 | async-start | bytes 7077888 | tf_op jit(solution)/shard_map/reduce_scatter | solution.py:270
  341.2 75.2 %copy-start.29 = (f32[64,2]{0,1:T(2,128)S(1)}, f32[64,2]{0,1:T(2,128)}, u32[]{:S(2)}) copy-start(f32[64,2]{0,1:T(2,128)} %param.45) | copy-start | bytes 1540
  412.6 17.2 %copy-start.8 = (bf16[64,2048]{1,0:T(8,128)(2,1)S(1)}, bf16[64,2048]{1,0:T(8,128)(2,1)}, u32[]{:S(2)}) copy-start(bf16[64,2048]{1,0:T(8,128)(2,1)} %reduce-scatter.3.cloned.1.call-done) | copy-start | bytes 786436
  412.6 12.9 %all-to-all-start.1 = ((bf16[96,2,2048]{2,1,0:T(2,128)(2,1)}), bf16[96,2,2048]{2,1,0:T(2,128)(2,1)S(1)}, u32[]{:S(2)}, u32[]{:S(2)}) async-start(bf16[96,2,2048]{2,1,0:T(2,128)(2,1)} %copy.215), calls=%async_computation.3 | async-start | bytes 1572864 | tf_op jit(solution)/shard_map/all_to_all | solution.py:278
  416.4 14.2 %copy-start.1 = (bf16[512,2048]{1,0:T(8,128)(2,1)S(1)}, bf16[512,2048]{1,0:T(8,128)(2,1)}, u32[]{:S(2)}) copy-start(bf16[512,2048]{1,0:T(8,128)(2,1)} %param.39) | copy-start | bytes 6291460
Sparse Core Ops, SparseCore 0:
  203.2 36.2 reduce-scatter.2
  255.7 63.9 all-gather.7
  341.3 68.3 reduce-scatter.4
where the time goes:
time: 441 us; the launch traced here: 437 us
  waiting for transfers between devices  177 us (40%)
  local copies, waits for them, and re-layouts  76.9 us (17%)
  other arithmetic  57.6 us (13%)
  blocking collectives  50.7 us (11%)
  matrix products  50.2 us (11%)
  between operations  13.7 us (3%)
  starting transfers between devices  11 us (2%)
    reduce_scatter x1, waiting for transfers between devices, per_device(): lax.psum_scatter(jnp.einsum('ref,efd->red', hidden, specialist_contract_m...  68.5 us
    all_gather x1, waiting for transfers between devices, per_device(): data_block = lax.all_gather(received, 'tp', axis=0, tiled=True)  63.8 us
    all_gather x4, blocking collectives, prefix(): lax.all_gather(part.astype(kind), axis)  38.7 us
    reduce_scatter x1, waiting for transfers between devices, per_device(): lax.psum_scatter(jnp.dot(mixed_rows, blend_result_matrix, preferred_eleme...  35.4 us
    dot_general x1, matrix products, per_device(): jnp.einsum('ref,efd->red', hidden, specialist_contract_matrix, preferred_...  12.5 us
    all_to_all x1, blocking collectives, per_device(): lax.all_to_all(buffer, 'sp', split_axis=1, concat_axis=0, tiled=True)  12 us
    dot_general x2, matrix products, local_sweep(): jnp.einsum('gkbij,bjgkp->bigkp', mixing, values, precision=HIGHEST_MODE)  11.3 us
    mul x3, other arithmetic, centred_conv(): return jax.nn.silu(summed)  9.7 us
  transfers between devices with their start and end apart: 6, of which 4 were waited for; matrix products, arithmetic and copies ran while one was open for 6% of the time, Pallas kernels for 0%

commit v1 on v0

--- a/solution.py
+++ b/solution.py
@@ -259,7 +259,15 @@
     ).astype(jnp.bfloat16)
     buffer = buffer.reshape(capacity, expert_count, WIDTH)
     received = lax.all_to_all(buffer, "sp", split_axis=1, concat_axis=0, tiled=True)
-    data_block = lax.all_gather(received, "tp", axis=0, tiled=True)
+    count_2 = lax.axis_size("tp")
+    current, shards = (received, [received])
+    for _ in range(count_2 - 1):
+        current = lax.ppermute(
+            current, "tp", [(i_2, (i_2 + 1) % count_2) for i_2 in range(count_2)]
+        )
+        shards.insert(0, current)
+    line = jnp.concatenate(shards, axis=0)
+    data_block = jnp.roll(line, (lax.axis_index("tp") + 1) * received.shape[0], axis=0)
     gate_part = jnp.einsum(
         "red,edf->ref", data_block, specialist_switch_matrix, preferred_element_type=jnp.float32
     )

time: 441 us -> 489 us (1.11); the launches traced: 437 us -> 480 us
  waiting for transfers between devices: 177 us -> 204 us
  local copies, waits for them, and re-layouts: 76.9 us -> 91.8 us
    ppermute x0 -> x7, waiting for transfers between devices: none -> 92.8 us  [per_device(): lax.ppermute(current, 'tp', [(i_2, (i_2 + 1) % count_2) for i_2 in range(...]
    all_gather x1 -> x0, waiting for transfers between devices: 63.8 us -> none  [per_device(): data_block = lax.all_gather(received, 'tp', axis=0, tiled=True)]
    unnamed x68 -> x81, local copies, waits for them, and re-layouts: 5.77 us -> 21 us
  transfers between devices with their start and end apart: 6 -> 12, of which waited for: 4 -> 10; matrix products, arithmetic and copies ran while one was open for 6% -> 6% of each run, Pallas kernels for 0% -> 0%
where the time goes in v1:
time: 489 us; the launch traced here: 480 us
  waiting for transfers between devices  204 us (42%)
  local copies, waits for them, and re-layouts  91.8 us (19%)
  other arithmetic  57.5 us (12%)
  blocking collectives  50.7 us (10%)
  matrix products  50.3 us (10%)
  between operations  14.3 us (3%)
  starting transfers between devices  10.8 us (2%)
    ppermute x7, waiting for transfers between devices, per_device(): lax.ppermute(current, 'tp', [(i_2, (i_2 + 1) % count_2) for i_2 in range(...  92.8 us
    reduce_scatter x1, waiting for transfers between devices, per_device(): lax.psum_scatter(jnp.einsum('ref,efd->red', hidden, specialist_contract_m...  66.6 us
    all_gather x4, blocking collectives, prefix(): lax.all_gather(part.astype(kind), axis)  38.8 us
    reduce_scatter x1, waiting for transfers between devices, per_device(): lax.psum_scatter(jnp.dot(mixed_rows, blend_result_matrix, preferred_eleme...  35.4 us
    unnamed x81, local copies, waits for them, and re-layouts  21 us
    dot_general x1, matrix products, per_device(): jnp.einsum('ref,efd->red', hidden, specialist_contract_matrix, preferred_...  12.3 us
    all_to_all x1, blocking collectives, per_device(): lax.all_to_all(buffer, 'sp', split_axis=1, concat_axis=0, tiled=True)  11.9 us
    dot_general x2, matrix products, local_sweep(): jnp.einsum('gkbij,bjgkp->bigkp', mixing, values, precision=HIGHEST_MODE)  11.1 us
  transfers between devices with their start and end apart: 12, of which 10 were waited for; matrix products, arithmetic and copies ran while one was open for 6% of the time, Pallas kernels for 0%

profile of v1, /device:TPU:0, one launch (start us, length us, event | category | flops | bytes accessed | tf_op | source)
XLA Modules:
  0.0 479.5 jit_solution(2227715818287565500)
XLA Ops:
  9.1 5.6 %collective-permute-start = (bf16[2,1024]{0,1:T(8,128)(2,1)}, bf16[2,1024]{0,1:T(8,128)(2,1)}, u32[]{:S(2)}, u32[]{:S(2)}) collective-permute-start(bf16[2,1024]{0,1:T(8,128)(2,1)} %copy.175), channel_id=1, source_target_pairs={{0,8},{8,16},{16,24},{1,9},{9,17},{17,25},{2,10},{10,18},{18,26},{... | collective-permute-start | bytes 12296 | tf_op jit(solution)/shard_map/ppermute | solution.py:23
  22.8 2.4 reduce_window_sum.45
  27.1 2.4 reduce_window_sum.47
  30.8 9.9 %all-gather.4 = bf16[4,2,4]{2,1,0:T(2,128)(2,1)} all-gather(bf16[1,2,4]{2,1,0:T(2,128)(2,1)S(1)} %bitcast.210), channel_id=2, replica_groups=mesh['sp'=4,'tp'=8] {'sp'}, dimensions={0}, use_global_device_ids=true | all-gather | bytes 80 | tf_op jit(solution)/shard_map/all_gather | solution.py:34
  40.7 7.4 %all-gather.5 = bf16[4,2,4]{2,1,0:T(2,128)(2,1)} all-gather(bf16[1,2,4]{2,1,0:T(2,128)(2,1)S(1)} %bitcast.211), channel_id=4, replica_groups=mesh['sp'=4,'tp'=8] {'sp'}, dimensions={0}, use_global_device_ids=true | all-gather | bytes 80 | tf_op jit(solution)/shard_map/all_gather | solution.py:34
  62.0 3.0 divide_multiply_fusion.2
  65.0 2.1 reshape.175
  67.1 4.7 rev.24
  76.7 4.7 rev.25
  83.3 4.7 divide_multiply_fusion
  88.0 2.6 reshape.174
  90.6 9.4 %rev.21 = f32[512,512]{0,1:T(8,128)} reverse(f32[512,512]{0,1:T(8,128)} %divide_multiply_fusion), dimensions={0} | reverse | bytes 2097152 | tf_op jit(solution)/shard_map/jit(_flip)/rev | solution.py:140
  99.9 3.2 fusion.79
  104.6 3.1 fusion.47
  108.8 9.8 %while.56 = (s32[]{:T(128)}, f32[2,4,64,128]{3,2,1,0:T(8,128)S(1)}, f32[4,2,4,64,128]{4,3,2,1,0:T(8,128)}, f32[4,2,4]{2,1,0:T(2,128)}, f32[4,2,4,64,128]{4,3,2,1,0:T(8,128)}, /*index=5*/s32[]{:T(128)}, s32[]{:T(128)}) while((s32[]{:T(128)}, f32[2,4,64,128]{3,2,1,0:T(8,128)S(1)}, f32[4,2,4,64,128]{4,3,2,1,0:T(8,128)}, ...), condition=%wide.region_2.3_spmd.clone, body=%wide.region_1.2_spmd.clone.sunk | while | flops 262147 | bytes 1311424 | solution.py:96
  118.6 11.2 %all-gather.1 = bf16[8,4,64,128]{3,2,1,0:T(8,128)(2,1)} all-gather(bf16[2,4,64,128]{3,2,1,0:T(8,128)(2,1)S(1)} %convert_element_type.229), channel_id=3, replica_groups=mesh['sp'=4,'tp'=8] {'sp'}, dimensions={0}, use_global_device_ids=true | all-gather | bytes 655360 | tf_op jit(solution)/shard_map/all_gather | solution.py:34
  129.8 6.7 %while.57 = (s32[]{:T(128)}, f32[2,4,64,128]{3,2,1,0:T(8,128)S(1)}, s32[]{:T(128)}, bf16[4,2,4]{2,1,0:T(2,128)(2,1)}, bf16[4,2,4,64,128]{4,3,2,1,0:T(8,128)(2,1)}, /*index=5*/s32[]{:T(128)}, s32[]{:T(128)}) while((s32[]{:T(128)}, f32[2,4,64,128]{3,2,1,0:T(8,128)S(1)}, s32[]{:T(128)}, bf16[4,2,4]{2,1,0:T(2,128)(2,1)}, ...), condition=%wide.region_5.6_spmd.clone, body=%wide.region_4.5_spmd.clone.sunk | while | flops 327692 | bytes 655545 | solution.py:52
  136.6 5.5 %fusion.25 = f32[4,128,2,4,64]{1,4,3,2,0:T(8,128)S(1)} fusion(f32[4,128,2,4,64]{1,0,4,3,2:T(4,128)} %reshape.174, f32[2,4,128,128]{3,2,0,1:T(8,128)} %fusion.79, f32[2,4,4,128]{3,1,0,2:T(4,128)S(1)} %bitcast.194, f32[2,4,4,128]{3,1,0,2:T(4,128)S(1)} %copy-done.24, pred[128,128]{1,0:T(8,128)(4,1)S(1)} %copy-done.22), kind=kOutput, calls=%fused_computation.40 | convolution fusion | flops 404750336 | bytes 2670592 | tf_op jit(solution)/shard_map/gkbij,bjgkp->bigkp/dot_general | solution.py:84
  142.2 2.5 fusion.34
  147.6 2.1 reshape.181
  149.7 2.5 reshape.178
  152.3 3.1 fusion.76
  156.7 3.1 fusion.44
  161.0 9.7 %while.58 = (s32[]{:T(128)}, f32[2,4,64,128]{3,2,1,0:T(8,128)S(1)}, f32[4,2,4,64,128]{4,3,2,1,0:T(8,128)}, f32[4,2,4]{2,1,0:T(2,128)}, f32[4,2,4,64,128]{4,3,2,1,0:T(8,128)}, /*index=5*/s32[]{:T(128)}, s32[]{:T(128)}) while((s32[]{:T(128)}, f32[2,4,64,128]{3,2,1,0:T(8,128)S(1)}, f32[4,2,4,64,128]{4,3,2,1,0:T(8,128)}, ...), condition=%wide.region_9.10_spmd.clone, body=%wide.region_8.9_spmd.clone.sunk | while | flops 262147 | bytes 1311424 | solution.py:96
  170.8 10.3 %all-gather.3 = bf16[8,4,64,128]{3,2,1,0:T(8,128)(2,1)} all-gather(bf16[2,4,64,128]{3,2,1,0:T(8,128)(2,1)S(1)} %convert_element_type.232), channel_id=5, replica_groups=mesh['sp'=4,'tp'=8] {'sp'}, dimensions={0}, use_global_device_ids=true | all-gather | bytes 655360 | tf_op jit(solution)/shard_map/all_gather | solution.py:34
  181.1 6.7 %while.59 = (s32[]{:T(128)}, f32[2,4,64,128]{3,2,1,0:T(8,128)S(1)}, s32[]{:T(128)}, bf16[4,2,4]{2,1,0:T(2,128)(2,1)}, bf16[4,2,4,64,128]{4,3,2,1,0:T(8,128)(2,1)...) while((s32[]{:T(128)}, f32[2,4,64,128]{3,2,1,0:T(8,128)S(1)}, s32[]{:T(128)}, ...), condition=%wide.region_12.13_spmd.clone, body=%wide.region_11.12_spmd.clone.sunk | while | flops 327696 | bytes 655607 | solution.py:52
  187.8 5.5 %fusion.28 = f32[4,128,2,4,64]{1,4,3,2,0:T(8,128)S(1)} fusion(f32[4,128,2,4,64]{1,0,4,3,2:T(4,128)} %reshape.178, f32[2,4,128,128]{3,2,0,1:T(8,128)} %fusion.76, f32[2,4,4,128]{3,1,0,2:T(4,128)S(1)} %bitcast.193, f32[2,4,4,128]{3,1,0,2:T(4,128)S(1)} %copy-done.23, pred[128,128]{1,0:T(8,128)(4,1)S(1)} %copy-done.22), kind=kOutput, calls=%fused_computation.41 | convolution fusion | flops 404750336 | bytes 2670592 | tf_op jit(solution)/shard_map/gkbij,bjgkp->bigkp/dot_general | solution.py:84
  193.4 2.5 fusion.32
  196.6 6.0 %rev.26 = f32[512,512]{0,1:T(8,128)} reverse(f32[512,512]{0,1:T(8,128)S(1)} %bitcast.184), dimensions={0} | reverse | bytes 2097152 | tf_op jit(solution)/shard_map/jit(_flip)/rev | solution.py:225
  202.6 2.1 bitcast_reduce_fusion
  205.0 2.6 convolution_convert_fusion
  208.7 35.4 %reduce-scatter.3.cloned.1.call-done = bf16[64,2048]{1,0:T(8,128)(2,1)} async-done(((bf16[512,2048]{1,0:T(8,128)(2,1)}), bf16[64,2048]{1,0:T(8,128)(2,1)}) %reduce-scatter.3.cloned.1.call-update) | async-done | bytes 262160 | tf_op jit(solution)/shard_map/reduce_scatter | solution.py:230
  247.1 11.9 %all_to_all.33 = bf16[24,8,2048]{2,0,1:T(8,128)(2,1)S(1)} all-to-all(bf16[24,8,2048]{2,0,1:T(8,128)(2,1)S(1)} %copy.213), channel_id=1, replica_groups=mesh['sp'=4,'tp'=8] {'sp'}, dimensions={1} | all-to-all | bytes 1572864 | tf_op jit(solution)/shard_map/all_to_all | solution.py:261
  259.1 13.2 %collective-permute-done.2 = bf16[96,2,2048]{2,0,1:T(8,128)(2,1)S(1)} collective-permute-done((bf16[96,2,2048]{2,0,1:T(8,128)(2,1)S(1)}, bf16[96,2,2048]{2,0,1:T(8,128)(2,1)S(1)}, u32[]{:S(2)}, u32[]{:S(2)}) %collective-permute-start.2) | collective-permute-done | bytes 786464 | tf_op jit(solution)/shard_map/ppermute | solution.py:265
  272.3 13.2 %collective-permute-done.3 = bf16[96,2,2048]{2,0,1:T(8,128)(2,1)S(1)} collective-permute-done((bf16[96,2,2048]{2,0,1:T(8,128)(2,1)S(1)}, bf16[96,2,2048]{2,0,1:T(8,128)(2,1)S(1)}, u32[]{:S(2)}, u32[]{:S(2)}) %collective-permute-start.3) | collective-permute-done | bytes 786464 | tf_op jit(solution)/shard_map/ppermute | solution.py:265
  285.5 13.2 %collective-permute-done.4 = bf16[96,2,2048]{2,0,1:T(8,128)(2,1)S(1)} collective-permute-done((bf16[96,2,2048]{2,0,1:T(8,128)(2,1)S(1)}, bf16[96,2,2048]{2,0,1:T(8,128)(2,1)S(1)}, u32[]{:S(2)}, u32[]{:S(2)}) %collective-permute-start.4) | collective-permute-done | bytes 786464 | tf_op jit(solution)/shard_map/ppermute | solution.py:265
  299.6 13.2 %collective-permute-done.5 = bf16[96,2,2048]{2,0,1:T(8,128)(2,1)S(1)} collective-permute-done((bf16[96,2,2048]{2,0,1:T(8,128)(2,1)S(1)}, bf16[96,2,2048]{2,0,1:T(8,128)(2,1)S(1)}, u32[]{:S(2)}, u32[]{:S(2)}) %collective-permute-start.5) | collective-permute-done | bytes 786464 | tf_op jit(solution)/shard_map/ppermute | solution.py:265
  313.7 13.2 %collective-permute-done.6 = bf16[96,2,2048]{2,0,1:T(8,128)(2,1)S(1)} collective-permute-done((bf16[96,2,2048]{2,0,1:T(8,128)(2,1)S(1)}, bf16[96,2,2048]{2,0,1:T(8,128)(2,1)S(1)}, u32[]{:S(2)}, u32[]{:S(2)}) %collective-permute-start.6) | collective-permute-done | bytes 786464 | tf_op jit(solution)/shard_map/ppermute | solution.py:265
  327.9 13.3 %collective-permute-done.7 = bf16[96,2,2048]{2,0,1:T(8,128)(2,1)} collective-permute-done((bf16[96,2,2048]{2,0,1:T(8,128)(2,1)S(1)}, bf16[96,2,2048]{2,0,1:T(8,128)(2,1)}, u32[]{:S(2)}, u32[]{:S(2)}) %collective-permute-start.7) | collective-permute-done | bytes 786464 | tf_op jit(solution)/shard_map/ppermute | solution.py:265
  341.4 13.5 %collective-permute-done.8 = bf16[96,2,2048]{2,0,1:T(8,128)(2,1)} collective-permute-done((bf16[96,2,2048]{2,0,1:T(8,128)(2,1)}, bf16[96,2,2048]{2,0,1:T(8,128)(2,1)}, u32[]{:S(2)}, u32[]{:S(2)}) %collective-permute-start.8) | collective-permute-done | bytes 786464 | tf_op jit(solution)/shard_map/ppermute | solution.py:265
  363.2 4.5 copy-done.19
  367.7 5.1 %fusion.4 = f32[2,768,512]{2,1,0:T(8,128)} fusion(bf16[2,2048,512]{2,1,0:T(8,128)(2,1)S(1)} %copy-done.29, bf16[1536,2,2048]{2,0,1:T(8,128)(2,1)S(1)} %constant_dynamic-update-slice_fusion, s32[]{:T(128)S(6)} %select_n.81), kind=kOutput, calls=%fused_computation.15 | convolution fusion | flops 3221225472 | bytes 13631492 | tf_op jit(solution)/shard_map/red,edf->ref/dot_general | solution.py:271
  372.8 12.3 %convert_bitcast_fusion = bf16[768,2,2048]{2,0,1:T(8,128)(2,1)} fusion(bf16[2,512,2048]{2,1,0:T(8,128)(2,1)} %param.43, f32[2,768,512]{2,1,0:T(8,128)} %fusion.4, bf16[2,2048,512]{2,1,0:T(8,128)(2,1)} %param.42, bf16[1536,2,2048]{2,0,1:T(8,128)(2,1)} %copy-done.19, s32[]{:T(128)S(6)} %select_n.81), kind=kOutput, calls=%fused_computation.12 | convolution fusion | flops 6450315264 | bytes 24117252 | tf_op jit(solution)/shard_map/ref,efd->red/dot_general | solution.py:279
  385.2 66.6 %reduce-scatter.5.cloned.1.call-done = bf16[96,2,2048]{2,0,1:T(8,128)(2,1)} async-done(((bf16[768,2,2048]{2,0,1:T(8,128)(2,1)}), bf16[96,2,2048]{2,0,1:T(8,128)(2,1)}) %reduce-scatter.5.cloned.1.call-update) | async-done | bytes 786448 | tf_op jit(solution)/shard_map/reduce_scatter | solution.py:278
  451.8 2.9 copy.215
  454.6 3.6 all-to-all-start.1
  458.3 9.1 %all-to-all-done.1 = bf16[96,2,2048]{2,1,0:T(2,128)(2,1)S(1)} async-done(((bf16[96,2,2048]{2,1,0:T(2,128)(2,1)}), bf16[96,2,2048]{2,1,0:T(2,128)(2,1)S(1)}, u32[]{:S(2)}, u32[]{:S(2)}) %all-to-all-start.1) | async-done | bytes 786464 | tf_op jit(solution)/shard_map/all_to_all | solution.py:286
  469.1 2.3 reshape.218
  (212 shorter events, 94.1 us)
Async XLA Ops:
  6.5 198.4 %copy-start = (bf16[512,2048]{1,0:T(8,128)(2,1)S(1)}, bf16[512,2048]{1,0:T(8,128)(2,1)}, u32[]{:S(2)}) copy-start(bf16[512,2048]{1,0:T(8,128)(2,1)} %param.39) | copy-start | bytes 6291460
  6.5 66.1 %copy-start.11 = (bf16[512,256]{1,0:T(8,128)(2,1)S(1)}, bf16[512,256]{1,0:T(8,128)(2,1)}, u32[]{:S(2)}) copy-start(bf16[512,256]{1,0:T(8,128)(2,1)} %param.30) | copy-start | bytes 786436
  6.5 237.6 %reduce-scatter.3.cloned.1.call-start = ((), (), s32[]{:S(2)}) async-start(), calls=%async_computation.4 | async-start | bytes 2359296 | tf_op jit(solution)/shard_map/reduce_scatter | solution.py:230
  9.1 48.3 %collective-permute-start = (bf16[2,1024]{0,1:T(8,128)(2,1)}, bf16[2,1024]{0,1:T(8,128)(2,1)}, u32[]{:S(2)}, u32[]{:S(2)}) collective-permute-start(bf16[2,1024]{0,1:T(8,128)(2,1)} %copy.175), channel_id=1, source_target_pairs={{0,8},{8,16},{16,24},{1,9},{9,17},{17,25},{2,10},{10,18},{18,26},{... | collective-permute-start | bytes 12296 | tf_op jit(solution)/shard_map/ppermute | solution.py:23
  15.5 43.4 %collective-permute-start.1 = (bf16[2,1024]{0,1:T(8,128)(2,1)}, bf16[2,1024]{0,1:T(8,128)(2,1)}, u32[]{:S(2)}, u32[]{:S(2)}) collective-permute-start(bf16[2,1024]{0,1:T(8,128)(2,1)} %copy.178), channel_id=1, source_target_pairs={{8,0},{16,8},{24,16},{9,1},{17,9},{25,17},{10,2},{18,10},{26,18},{... | collective-permute-start | bytes 12296 | tf_op jit(solution)/shard_map/ppermute | solution.py:26
  22.8 3.7 copy-start.17
  27.1 2.6 copy-start.15
  72.5 30.6 %copy-start.12 = (f32[4,128,2,4]{1,0,3,2:T(4,128)S(1)}, f32[4,128,2,4]{1,0,3,2:T(4,128)}, u32[]{:S(2)}) copy-start(f32[4,128,2,4]{1,0,3,2:T(4,128)} %get-tuple-element.476) | copy-start | bytes 49156
  107.7 28.9 %copy-start.18 = (f32[1,8,512]{2,1,0:T(8,128)S(1)}, f32[1,8,512]{2,1,0:T(8,128)}, u32[]{:S(2)}) copy-start(f32[1,8,512]{2,1,0:T(8,128)} %copy-done.17) | copy-start | bytes 49156
  107.7 28.9 %copy-start.22 = (pred[128,128]{1,0:T(8,128)(4,1)S(1)}, pred[128,128]{1,0:T(8,128)(4,1)}, u32[]{:S(2)}) copy-start(pred[128,128]{1,0:T(8,128)(4,1)} %iota_compare_fusion.3) | copy-start | bytes 49156
  107.7 28.9 %copy-start.24 = (f32[2,4,4,128]{3,1,0,2:T(4,128)S(1)}, f32[2,4,4,128]{3,1,0,2:T(4,128)}, u32[]{:S(2)}) copy-start(f32[2,4,4,128]{3,1,0,2:T(4,128)} %copy.180) | copy-start | bytes 49156
  108.8 33.4 %copy-start.14 = (f32[4,128,2,4]{1,3,2,0:T(4,128)S(1)}, f32[4,128,2,4]{1,3,2,0:T(4,128)}, u32[]{:S(2)}) copy-start(f32[4,128,2,4]{1,3,2,0:T(4,128)} %copy.195) | copy-start | bytes 49156
  108.8 33.4 %copy-start.21 = (f32[4,2,4]{2,1,0:T(2,128)S(1)}, f32[4,2,4]{2,1,0:T(2,128)}, u32[]{:S(2)}) copy-start(f32[4,2,4]{2,1,0:T(2,128)} %copy.193) | copy-start | bytes 388
  118.6 23.6 %copy-start.2 = (f32[4,128,2,128]{3,2,1,0:T(2,128)S(1)}, f32[4,128,2,128]{3,2,1,0:T(2,128)}, u32[]{:S(2)}) copy-start(f32[4,128,2,128]{3,2,1,0:T(2,128)} %reshape.175) | copy-start | bytes 1572868
  159.8 28.0 %copy-start.16 = (f32[8,512]{1,0:T(8,128)S(1)}, f32[8,512]{1,0:T(8,128)}, u32[]{:S(2)}) copy-start(f32[8,512]{1,0:T(8,128)} %copy-done.15) | copy-start | bytes 49156
  159.8 28.0 %copy-start.23 = (f32[2,4,4,128]{3,1,0,2:T(4,128)S(1)}, f32[2,4,4,128]{3,1,0,2:T(4,128)}, u32[]{:S(2)}) copy-start(f32[2,4,4,128]{3,1,0,2:T(4,128)} %copy.197) | copy-start | bytes 49156
  161.0 32.4 %copy-start.13 = (f32[4,128,2,4]{1,3,2,0:T(4,128)S(1)}, f32[4,128,2,4]{1,3,2,0:T(4,128)}, u32[]{:S(2)}) copy-start(f32[4,128,2,4]{1,3,2,0:T(4,128)} %copy.208) | copy-start | bytes 49156
  161.0 32.4 %copy-start.20 = (f32[4,2,4]{2,1,0:T(2,128)S(1)}, f32[4,2,4]{2,1,0:T(2,128)}, u32[]{:S(2)}) copy-start(f32[4,2,4]{2,1,0:T(2,128)} %copy.206) | copy-start | bytes 388
  193.4 11.4 %copy-start.28 = (f32[512]{0:T(512)S(1)}, f32[512]{0:T(512)}, u32[]{:S(2)}) copy-start(f32[512]{0:T(512)} %param.38) | copy-start | bytes 6148
  202.6 5.1 %copy-start.26 = (s32[64,2]{0,1:T(2,128)S(1)}, s32[64,2]{0,1:T(2,128)}, u32[]{:S(2)}) copy-start(s32[64,2]{0,1:T(2,128)} %param.44) | copy-start | bytes 1540
  202.6 41.5 %copy-start.9 = (bf16[64,2048]{1,0:T(8,128)(2,1)S(1)}, bf16[64,2048]{1,0:T(8,128)(2,1)}, u32[]{:S(2)}) copy-start(bf16[64,2048]{1,0:T(8,128)(2,1)} %param.27) | copy-start | bytes 786436
  202.6 42.7 %copy-start.25 = (f32[2048]{0:T(1024)S(1)}, f32[2048]{0:T(1024)}, u32[]{:S(2)}) copy-start(f32[2048]{0:T(1024)} %param.40) | copy-start | bytes 24580
  207.6 244.1 %reduce-scatter.5.cloned.1.call-start = ((), (), s32[]{:S(2)}) async-start(), calls=%async_computation.5 | async-start | bytes 7077888 | tf_op jit(solution)/shard_map/reduce_scatter | solution.py:278
  259.0 13.3 %collective-permute-start.2 = (bf16[96,2,2048]{2,0,1:T(8,128)(2,1)S(1)}, bf16[96,2,2048]{2,0,1:T(8,128)(2,1)S(1)}, u32[]{:S(2)}, u32[]{:S(2)}) collective-permute-start(bf16[96,2,2048]{2,0,1:T(8,128)(2,1)S(1)} %bitcast.176), channel_id=1, source_target_pairs={{0,1},{1,2},{2,3},{3,4},{4,5},{5,6},{6,7},{7,0},{8,9},{9,10},{10,1... | collective-permute-start | bytes 2359304 | tf_op jit(solution)/shard_map/ppermute | solution.py:265
  272.3 13.2 %collective-permute-start.3 = (bf16[96,2,2048]{2,0,1:T(8,128)(2,1)S(1)}, bf16[96,2,2048]{2,0,1:T(8,128)(2,1)S(1)}, u32[]{:S(2)}, u32[]{:S(2)}) collective-permute-start(bf16[96,2,2048]{2,0,1:T(8,128)(2,1)S(1)} %collective-permute-done.2), channel_id=1, source_target_pairs={{0,1},{1,2},{2,3},{3,4},{4,5},{5,6},{6,7},{7,0},{8,9},{9,10},{10,1... | collective-permute-start | bytes 2359304 | tf_op jit(solution)/shard_map/ppermute | solution.py:265
  285.5 13.2 %collective-permute-start.4 = (bf16[96,2,2048]{2,0,1:T(8,128)(2,1)S(1)}, bf16[96,2,2048]{2,0,1:T(8,128)(2,1)S(1)}, u32[]{:S(2)}, u32[]{:S(2)}) collective-permute-start(bf16[96,2,2048]{2,0,1:T(8,128)(2,1)S(1)} %collective-permute-done.3), channel_id=1, source_target_pairs={{0,1},{1,2},{2,3},{3,4},{4,5},{5,6},{6,7},{7,0},{8,9},{9,10},{10,1... | collective-permute-start | bytes 2359304 | tf_op jit(solution)/shard_map/ppermute | solution.py:265
  298.7 0.9 copy-start.3
  299.6 13.2 %collective-permute-start.5 = (bf16[96,2,2048]{2,0,1:T(8,128)(2,1)S(1)}, bf16[96,2,2048]{2,0,1:T(8,128)(2,1)S(1)}, u32[]{:S(2)}, u32[]{:S(2)}) collective-permute-start(bf16[96,2,2048]{2,0,1:T(8,128)(2,1)S(1)} %collective-permute-done.4), channel_id=1, source_target_pairs={{0,1},{1,2},{2,3},{3,4},{4,5},{5,6},{6,7},{7,0},{8,9},{9,10},{10,1... | collective-permute-start | bytes 2359304 | tf_op jit(solution)/shard_map/ppermute | solution.py:265
  312.8 0.9 copy-start.5
  313.7 13.2 %collective-permute-start.6 = (bf16[96,2,2048]{2,0,1:T(8,128)(2,1)S(1)}, bf16[96,2,2048]{2,0,1:T(8,128)(2,1)S(1)}, u32[]{:S(2)}, u32[]{:S(2)}) collective-permute-start(bf16[96,2,2048]{2,0,1:T(8,128)(2,1)S(1)} %collective-permute-done.5), channel_id=1, source_target_pairs={{0,1},{1,2},{2,3},{3,4},{4,5},{5,6},{6,7},{7,0},{8,9},{9,10},{10,1... | collective-permute-start | bytes 2359304 | tf_op jit(solution)/shard_map/ppermute | solution.py:265
  327.0 0.9 copy-start.7
  327.9 13.3 %collective-permute-start.7 = (bf16[96,2,2048]{2,0,1:T(8,128)(2,1)S(1)}, bf16[96,2,2048]{2,0,1:T(8,128)(2,1)}, u32[]{:S(2)}, u32[]{:S(2)}) collective-permute-start(bf16[96,2,2048]{2,0,1:T(8,128)(2,1)S(1)} %collective-permute-done.6), channel_id=1, source_target_pairs={{0,1},{1,2},{2,3},{3,4},{4,5},{5,6},{6,7},{7,0},{8,9},{9,10},{10,1... | collective-permute-start | bytes 2359304 | tf_op jit(solution)/shard_map/ppermute | solution.py:265
  341.2 13.7 %collective-permute-start.8 = (bf16[96,2,2048]{2,0,1:T(8,128)(2,1)}, bf16[96,2,2048]{2,0,1:T(8,128)(2,1)}, u32[]{:S(2)}, u32[]{:S(2)}) collective-permute-start(bf16[96,2,2048]{2,0,1:T(8,128)(2,1)} %collective-permute-done.7), channel_id=1, source_target_pairs={{0,1},{1,2},{2,3},{3,4},{4,5},{5,6},{6,7},{7,0},{8,9},{9,10},{10,1... | collective-permute-start | bytes 2359304 | tf_op jit(solution)/shard_map/ppermute | solution.py:265
  341.4 18.4 %copy-start.4 = (bf16[96,2,2048]{2,0,1:T(8,128)(2,1)S(1)}, bf16[96,2,2048]{2,0,1:T(8,128)(2,1)}, u32[]{:S(2)}) copy-start(bf16[96,2,2048]{2,0,1:T(8,128)(2,1)} %copy-done.3) | copy-start | bytes 2359300
  357.3 5.5 %copy-start.8 = (bf16[96,2,2048]{2,0,1:T(8,128)(2,1)S(1)}, bf16[96,2,2048]{2,0,1:T(8,128)(2,1)}, u32[]{:S(2)}) copy-start(bf16[96,2,2048]{2,0,1:T(8,128)(2,1)} %copy-done.7) | copy-start | bytes 2359300
  358.5 4.3 copy-start.6
  360.1 7.6 %copy-start.29 = (bf16[2,2048,512]{2,1,0:T(8,128)(2,1)S(1)}, bf16[2,2048,512]{2,1,0:T(8,128)(2,1)}, u32[]{:S(2)}) copy-start(bf16[2,2048,512]{2,1,0:T(8,128)(2,1)} %param.41) | copy-start | bytes 12582916
  363.2 4.5 copy-start.19
  385.1 73.1 %copy-start.27 = (f32[64,2]{0,1:T(2,128)S(1)}, f32[64,2]{0,1:T(2,128)}, u32[]{:S(2)}) copy-start(f32[64,2]{0,1:T(2,128)} %param.45) | copy-start | bytes 1540
  385.1 87.4 %copy-start.1 = (bf16[512,2048]{1,0:T(8,128)(2,1)S(1)}, bf16[512,2048]{1,0:T(8,128)(2,1)}, u32[]{:S(2)}) copy-start(bf16[512,2048]{1,0:T(8,128)(2,1)} %param.39) | copy-start | bytes 6291460
  385.1 86.6 %copy-start.10 = (bf16[64,2048]{1,0:T(8,128)(2,1)S(1)}, bf16[64,2048]{1,0:T(8,128)(2,1)}, u32[]{:S(2)}) copy-start(bf16[64,2048]{1,0:T(8,128)(2,1)} %reduce-scatter.3.cloned.1.call-done) | copy-start | bytes 786436
  454.6 12.7 %all-to-all-start.1 = ((bf16[96,2,2048]{2,1,0:T(2,128)(2,1)}), bf16[96,2,2048]{2,1,0:T(2,128)(2,1)S(1)}, u32[]{:S(2)}, u32[]{:S(2)}) async-start(bf16[96,2,2048]{2,1,0:T(2,128)(2,1)} %copy.215), calls=%async_computation.3 | async-start | bytes 1572864 | tf_op jit(solution)/shard_map/all_to_all | solution.py:286
Sparse Core Ops, SparseCore 0:
  207.7 36.3 reduce-scatter.2
  385.3 66.4 reduce-scatter.4
